TPU v7x, 32 devices: a whole 2x2x4 slice. The times are simulated.
32 devices in a mesh: ep: 8 (over z, x), tp: 4 (over y, core).
Axes of the slice: x: 2, y: 2, z: 4, core: 2. Of those that a mesh axis runs over, the one named last changes fastest.
Arguments:
- queries: bfloat16 [1024, 4096], P('ep', 'tp'), may hold values from -112 to 112
- key_rows: bfloat16 [1024, 4096], P('ep', 'tp'), may hold values from -8.1 to 8.1
- values: bfloat16 [1024, 4096], P('ep', 'tp'), may hold values from -6 to 6
- lambdas: float32 [16], P('tp'), may hold values from 0.3 to 0.8
- head_gain: float32 [256], replicated, may hold values from 0.1 to 1.9
- tokens: bfloat16 [512, 4096], P('ep'), may hold values from -6 to 6
- moe_gain: float32 [4096], replicated, may hold values from 0.1 to 1.9
- routes: int32 [512, 2], P('ep'), may hold values from 0 to 7, all different within a row; in each aligned block of 64 rows (0 to 63, 64 to 127, ...) at most 32 rows name the same one
- route_scores: float32 [512, 2], P('ep'), may hold values from -6 to 6
- w_gate: bfloat16 [8, 4096, 2048], P('ep', None, 'tp'), may hold values from -0.09375 to 0.09375
- w_up: bfloat16 [8, 4096, 2048], P('ep', None, 'tp'), may hold values from -0.09375 to 0.09375
- w_down: bfloat16 [8, 2048, 4096], P('ep', 'tp'), may hold values from -0.125 to 0.125
Outputs:
- attended: bfloat16 [1024, 4096], P('ep', 'tp')
- expert_out: bfloat16 [512, 4096], P('ep', 'tp')
Inputs may be any that keep to these rules, and one draw needn't show every extreme that they name: `routes`: each row names 2 different experts. Among the rows of one index of ep at most 32 name the same expert, and some index reaches 32 in every draw.
All inputs are finite; a program needn't handle non-finite values.
Results may differ from a plain program's by a relative error of at most 0.018.
Values may be sent and summed in bfloat16 or wider, within the bound.
A program may use at most 64 MiB of HBM per device.

v0:
```python
import jax
import jax.numpy as jnp
from jax import lax
from jax.sharding import PartitionSpec as P

QKD = 128
VD = 256
TOP = 2
neg_big = -1e30
head_eps = 1e-05
moe_eps = 1e-06
head_scale = 0.8


def slot_table(routes, experts, capacity):
    flat_routes = routes.reshape(-1)
    onehot = (flat_routes[:, None] == jnp.arange(experts, dtype=jnp.int32)[None, :]).astype(
        jnp.int32
    )
    before = jnp.cumsum(onehot, axis=0) - onehot
    position = jnp.sum(before * onehot, axis=1)
    return (flat_routes * capacity + position).reshape(routes.shape)


def fold_block(state, query_group, query_pos, key_heads, value_heads, key_pos):
    maxima, denominators, accumulated = state
    scores = jnp.einsum(
        "qhmd,khmd->hmqk", query_group, key_heads, preferred_element_type=jnp.float32
    ) * QKD ** (-0.5)
    visible = key_pos[None, :] <= query_pos[:, None]
    scores = jnp.where(visible, scores, neg_big)
    new_max = jnp.maximum(maxima, jnp.max(scores, axis=-1))
    weights = jnp.where(visible, jnp.exp(scores - new_max[..., None]), 0.0)
    accumulated = jnp.einsum(
        "hmqk,khd->hmqd", weights, value_heads, precision=lax.Precision.HIGHEST
    )
    denominators = jnp.sum(weights, axis=-1)
    return (new_max, denominators, accumulated)


def local(
    queries,
    key_rows,
    values,
    lambdas,
    head_gain,
    tokens,
    moe_gain,
    routes,
    route_scores,
    w_gate,
    w_up,
    w_down,
):
    rows_a = queries.shape[0]
    half_rows = rows_a // 2
    head_local = lambdas.shape[0]
    ep_count = lax.axis_size("ep")
    ep_index = lax.axis_index("ep")
    early_queries = queries[:half_rows]
    later_queries = queries[half_rows:]
    early_pos = ep_index * rows_a + jnp.arange(half_rows, dtype=jnp.int32)
    later_pos = ep_index * rows_a + half_rows + jnp.arange(half_rows, dtype=jnp.int32)
    query_groups = (
        early_queries.reshape(half_rows, head_local, 2, QKD),
        later_queries.reshape(half_rows, head_local, 2, QKD),
    )
    position_groups = (early_pos, later_pos)
    start_state = (
        jnp.full((head_local, 2, half_rows), neg_big, jnp.float32),
        jnp.zeros((head_local, 2, half_rows), jnp.float32),
        jnp.zeros((head_local, 2, half_rows, VD), jnp.float32),
    )
    totals = (start_state, start_state)
    row_start = jnp.int32(0)
    key_block = lax.all_gather(key_rows, "ep", axis=0, tiled=True)
    value_block = lax.all_gather(values, "ep", axis=0, tiled=True)
    key_count = key_block.shape[0]
    key_heads = key_block.reshape(key_count, head_local, 2, QKD)
    value_heads = value_block.reshape(key_count, head_local, VD).astype(jnp.float32)
    key_pos = jnp.arange(key_count, dtype=jnp.int32)
    updated = []
    for attend_group_index in range(2):
        state = totals[attend_group_index]
        query_group = query_groups[attend_group_index]
        query_pos = position_groups[attend_group_index]
        state = lax.cond(
            row_start <= query_pos[-1],
            lambda held: fold_block(held, query_group, query_pos, key_heads, value_heads, key_pos),
            lambda held: held,
            state,
        )
        updated.append(state)
    folded = (updated[0], updated[1])
    attended_groups = []
    for group_index in range(2):
        maxima, denominators, accumulated = folded[group_index]
        mixed_out = (
            accumulated[:, 0] / denominators[:, 0, :, None]
            - lambdas[:, None, None] * accumulated[:, 1] / denominators[:, 1, :, None]
        )
        scaled = mixed_out * lax.rsqrt(
            jnp.mean(mixed_out * mixed_out, axis=-1, keepdims=True) + head_eps
        )
        scaled = scaled * head_gain * head_scale
        attended_groups.append(
            scaled.transpose(1, 0, 2).reshape(half_rows, head_local * VD).astype(jnp.bfloat16)
        )
    later_out = attended_groups[1]
    attended = jnp.concatenate([attended_groups[0], later_out], axis=0)
    rows_b = tokens.shape[0]
    capacity = 2 * TOP * rows_b // ep_count
    token_f32 = tokens.astype(jnp.float32)
    normed = (
        token_f32
        * lax.rsqrt(jnp.mean(token_f32 * token_f32, axis=-1, keepdims=True) + moe_eps)
        * moe_gain
    ).astype(jnp.bfloat16)
    gate_weights = jax.nn.softmax(route_scores, axis=-1)
    slot_of = slot_table(routes, ep_count, capacity)
    row_ids = jnp.broadcast_to(jnp.arange(rows_b, dtype=jnp.int32)[:, None], slot_of.shape)
    row_of_slot = (
        jnp.zeros((ep_count * capacity,), jnp.int32)
        .at[slot_of.reshape(-1)]
        .set(row_ids.reshape(-1))
    )
    gate_local = w_gate[0]
    up_local = w_up[0]
    down_local = w_down[0]
    outgoing = normed[row_of_slot]
    arrived = lax.all_to_all(outgoing, "ep", split_axis=0, concat_axis=0, tiled=True)
    gate_act = jnp.dot(arrived, gate_local, preferred_element_type=jnp.float32)
    up_act = jnp.dot(arrived, up_local, preferred_element_type=jnp.float32)
    hidden = (jax.nn.silu(gate_act) * up_act).astype(jnp.bfloat16)
    summed = lax.psum_scatter(
        lax.dot_general(
            down_local, hidden, (((0,), (1,)), ((), ())), preferred_element_type=jnp.float32
        ).astype(jnp.bfloat16),
        "tp",
        scatter_dimension=0,
        tiled=True,
    )
    returned = lax.all_to_all(summed, "ep", split_axis=1, concat_axis=1, tiled=True)
    slot_ids = jnp.arange(ep_count * capacity, dtype=jnp.int32)
    combined = jnp.zeros((rows_b, returned.shape[0]), jnp.float32)
    for choice_index in range(TOP):
        picker = (slot_of[:, choice_index, None] == slot_ids[None, :]).astype(jnp.bfloat16)
        picked = lax.dot_general(
            picker, returned, (((1,), (1,)), ((), ())), preferred_element_type=jnp.float32
        )
        combined = combined + gate_weights[:, choice_index, None] * picked
    expert_out = combined.astype(jnp.bfloat16)
    return (attended, expert_out)


def solution(mesh):
    return jax.shard_map(
        local,
        mesh=mesh,
        in_specs=(
            P("ep", "tp"),
            P("ep", "tp"),
            P("ep", "tp"),
            P("tp"),
            P(),
            P("ep", None),
            P(),
            P("ep", None),
            P("ep", None),
            P("ep", None, "tp"),
            P("ep", None, "tp"),
            P("ep", "tp", None),
        ),
        out_specs=(P("ep", "tp"), P("ep", "tp")),
        check_vma=False,
    )
```

profile of v0, /device:TPU:0, one launch (start us, length us, event | category | flops | bytes accessed | tf_op | source)
XLA Modules:
  0.0 190.7 jit_solution(13893074613434656306)
XLA Ops:
  8.0 0.0 copy-start.2
  8.0 0.0 all-gather.5.cloned.1.call-start
  8.1 1.9 copy.24
  9.9 0.0 all-gather.5.cloned.1.call-update
  9.9 0.8 copy.34
  10.7 0.1 eq.45
  10.8 0.1 fusion.62
  10.9 0.2 reduce_window_sum.11
  11.1 0.2 select_reduce_fusion
  11.3 0.1 reduce_sum.71
  11.5 0.1 mul.157
  11.6 0.1 reshape.129
  11.8 1.0 scatter_custom_fusion
  12.8 1.2 fusion.42
  14.0 0.0 copy-done.2
  14.0 0.9 fusion.44
  15.0 3.2 %gather_fusion = bf16[256,4096]{1,0:T(8,128)(2,1)} fusion(bf16[64,4096]{1,0:T(8,128)(2,1)S(1)} %fusion.44, s32[1024]{0:T(1024)S(1)} %pad_clamp_fusion), kind=kCustom, calls=%fused_computation | custom fusion | bytes 4195328 | tf_op jit(solution)/shard_map/gather | solution.py:130
  18.2 7.4 %all-to-all-start = ((bf16[8,32,4096]{2,1,0:T(8,128)(2,1)}), bf16[8,32,4096]{2,1,0:T(8,128)(2,1)S(1)}, u32[]{:S(2)}, u32[]{:S(2)}) async-start(bf16[8,32,4096]{2,1,0:T(8,128)(2,1)} %bitcast.20), calls=%async_computation | async-start | bytes 4194304 | tf_op jit(solution)/shard_map/all_to_all | solution.py:131
  25.6 0.0 all-gather.3.cloned.1.call-start
  25.6 0.0 copy-done.3
  25.6 0.8 copy.23
  26.5 0.0 all-gather.3.cloned.1.call-update
  26.5 0.0 reduce-scatter.2.cloned.1.call-start
  26.5 69.8 %all-to-all-done = bf16[8,32,4096]{2,1,0:T(8,128)(2,1)S(1)} async-done(((bf16[8,32,4096]{2,1,0:T(8,128)(2,1)}), bf16[8,32,4096]{2,1,0:T(8,128)(2,1)S(1)}, u32[]{:S(2)}, u32[]{:S(2)}) %all-to-all-start) | async-done | bytes 2097184 | tf_op jit(solution)/shard_map/all_to_all | solution.py:131
  96.3 3.5 %fusion.32 = f32[256,512]{1,0:T(8,128)S(1)} fusion(bf16[256,4096]{1,0:T(8,128)(2,1)S(1)} %bitcast.99, bf16[1,4096,512]{2,1,0:T(8,128)(2,1)} %param.25), kind=kOutput, calls=%fused_computation.43 | convolution fusion | flops 1073741824 | bytes 6815744 | tf_op jit(solution)/shard_map/dot_general | solution.py:132
  99.8 7.4 %fusion.28 = bf16[4096,256]{0,1:T(8,128)(2,1)} fusion(bf16[1,512,4096]{2,1,0:T(8,128)(2,1)} %param.27, bf16[256,4096]{1,0:T(8,128)(2,1)S(1)} %bitcast.100, bf16[1,4096,512]{2,1,0:T(8,128)(2,1)} %param.26, f32[256,512]{1,0:T(8,128)S(1)} %fusion.32), kind=kOutput, calls=%fused_computation.39 | convolution fusion | flops 2149318656 | bytes 13107200 | tf_op jit(solution)/shard_map/dot_general | solution.py:136
  107.2 0.0 copy-start.5
  107.2 0.0 reduce-scatter.2.cloned.1.call-update
  107.2 0.6 slice.55
  108.5 0.6 slice.50
  109.7 0.0 copy-done.5
  109.8 0.2 slice_reduce_fusion
  110.0 0.0 all-gather.5.cloned.1.call-done
  110.0 0.0 copy-start.4
  110.0 4.1 %convert.3 = f32[1024,4,256]{0,2,1:T(8,128)} convert(bf16[1024,4,256]{0,2,1:T(8,128)(2,1)} %bitcast.98) | non-fusion elementwise | flops 1048576 | bytes 6291456 | tf_op jit(solution)/shard_map/convert_element_type | solution.py:80
  114.1 33.2 %all-gather.3.cloned.1.call-done = bf16[1024,1024]{0,1:T(8,128)(2,1)} async-done(((bf16[128,1024]{0,1:T(8,128)(2,1)}), bf16[1024,1024]{0,1:T(8,128)(2,1)}) %all-gather.3.cloned.1.call-update) | async-done | bytes 2097168 | tf_op jit(solution)/shard_map/all_gather | solution.py:76
  147.3 0.0 copy-done.4
  147.3 8.6 %conditional.3 = (f32[4,2,64]{2,1,0:T(2,128)S(1)}, f32[4,2,64,256]{3,2,1,0:T(8,128)S(1)}) conditional(s32[]{:T(128)} %bitcast.10, () %tuple.26, (s32[1024]{0:T(1024)S(1)}, s32[64]{0:T(128)S(1)}, bf16[128,1024]{1,0:T(8,128)(2,1)S(1)}, bf16[1024,4,2,128]{0,3,2,1:T(8,128)(2,1)}, f32[1024,4,256]{0,2,1:T(8,128)}) %tuple.56), branch_computations={%region_5.6_spmd, %region_6.9_spmd} | conditional | flops 1751186944 | bytes 30818604 | solution.py:87
  147.3 0.1 broadcast_compare_fusion.1
  147.4 0.1 reshape.109
  147.5 0.0 copy-start
  147.5 2.4 %fusion.16 = (f32[4,2,64]{2,1,0:T(2,128)S(1)}, f32[4,2,64,1024]{3,2,1,0:T(8,128)S(1)}) fusion(pred[64,1024]{1,0:T(8,128)(4,1)S(1)} %broadcast_compare_fusion.1, bf16[1024,4,2,128]{0,3,2,1:T(8,128)(2,1)} %get-tuple-element.52, bf16[64,4,2,128]{3,2,1,0:T(2,128)(2,1)S(1)} %reshape.109), kind=kOutput, calls=%fused_computation.24 | convolution fusion | flops 135790080 | bytes 4392960 | tf_op jit(solution)/shard_map/cond/branch_1_fun/qhmd,khmd->hmqk/dot_general | solution.py:27
  150.0 0.4 copy-done
  150.3 4.8 %fusion.14 = f32[4,2,64,256]{3,2,1,0:T(8,128)S(1)} fusion(f32[1024,4,256]{0,2,1:T(8,128)S(1)} %copy-done, f32[4,2,64,1024]{3,2,1,0:T(8,128)S(1)} %get-tuple-element.63, f32[4,2,64]{2,1,0:T(2,128)S(1)} %broadcast_maximum_fusion.1, pred[64,1024]{1,0:T(8,128)(4,1)S(1)} %broadcast_compare_fusion.1), kind=kOutput, calls=%fused_computation.20 | convolution fusion | flops 1612709888 | bytes 6883328 | tf_op jit(solution)/shard_map/cond/branch_1_fun/hmqk,khd->hmqd/dot_general | solution.py:34
  155.2 0.7 fusion.17
  155.9 0.0 copy-start.7
  155.9 8.8 %conditional.2 = (f32[4,2,64]{2,1,0:T(2,128)S(1)}, f32[4,2,64,256]{3,2,1,0:T(8,128)S(1)}) conditional(s32[]{:T(128)} %bitcast.2, () %tuple.24, (s32[1024]{0:T(1024)S(1)}, s32[64]{0:T(128)S(1)}, bf16[128,1024]{1,0:T(8,128)(2,1)S(1)}, bf16[1024,4,2,128]{0,3,2,1:T(8,128)(2,1)}, f32[1024,4,256]{0,2,1:T(8,128)}) %tuple.57), branch_computations={%region_0.0_spmd, %region_1.4_spmd} | conditional | flops 1751186944 | bytes 30818604 | solution.py:87
  156.1 0.1 broadcast_compare_fusion
  156.2 0.1 reshape.108
  156.3 0.0 copy-start.1
  156.3 2.4 %fusion.2 = (f32[4,2,64]{2,1,0:T(2,128)S(1)}, f32[4,2,64,1024]{3,2,1,0:T(8,128)S(1)}) fusion(pred[64,1024]{1,0:T(8,128)(4,1)S(1)} %broadcast_compare_fusion, bf16[1024,4,2,128]{0,3,2,1:T(8,128)(2,1)} %get-tuple-element.47, bf16[64,4,2,128]{3,2,1,0:T(2,128)(2,1)S(1)} %reshape.108), kind=kOutput, calls=%fused_computation.6 | convolution fusion | flops 135790080 | bytes 4392960 | tf_op jit(solution)/shard_map/cond/branch_1_fun/qhmd,khmd->hmqk/dot_general | solution.py:27
  158.7 0.4 copy-done.1
  159.1 4.8 %fusion = f32[4,2,64,256]{3,2,1,0:T(8,128)S(1)} fusion(f32[1024,4,256]{0,2,1:T(8,128)S(1)} %copy-done.1, f32[4,2,64,1024]{3,2,1,0:T(8,128)S(1)} %get-tuple-element.61, f32[4,2,64]{2,1,0:T(2,128)S(1)} %broadcast_maximum_fusion, pred[64,1024]{1,0:T(8,128)(4,1)S(1)} %broadcast_compare_fusion), kind=kOutput, calls=%fused_computation.2 | convolution fusion | flops 1612709888 | bytes 6883328 | tf_op jit(solution)/shard_map/cond/branch_1_fun/hmqk,khd->hmqd/dot_general | solution.py:34
  164.0 0.7 fusion.3
  164.7 0.0 reduce-scatter.2.cloned.1.call-done
  164.7 3.5 %all-to-all-start.1 = ((bf16[1024,8,32]{0,2,1:T(8,128)(2,1)}), bf16[1024,8,32]{0,2,1:T(8,128)(2,1)S(1)}, u32[]{:S(2)}, u32[]{:S(2)}) async-start(bf16[1024,8,32]{0,2,1:T(8,128)(2,1)} %bitcast.101), calls=%async_computation.2 | async-start | bytes 1048576 | tf_op jit(solution)/shard_map/all_to_all | solution.py:143
  168.2 0.0 copy-done.7
  168.3 0.4 multiply_reduce_fusion.1
  168.6 0.0 copy-done.6
  168.6 0.1 fusion.60
  168.8 0.7 pad_maximum_fusion
  169.5 12.6 %all-to-all-done.1 = bf16[1024,8,32]{0,2,1:T(8,128)(2,1)S(1)} async-done(((bf16[1024,8,32]{0,2,1:T(8,128)(2,1)}), bf16[1024,8,32]{0,2,1:T(8,128)(2,1)S(1)}, u32[]{:S(2)}, u32[]{:S(2)}) %all-to-all-start.1) | async-done | bytes 524320 | tf_op jit(solution)/shard_map/all_to_all | solution.py:143
  182.1 0.2 convolution_multiply_fusion.1
  182.4 0.9 fusion.41
  (25 shorter events, 0.2 us)
Async XLA Ops:
  8.0 6.0 %copy-start.2 = (bf16[64,4096]{1,0:T(8,128)(2,1)S(1)}, bf16[64,4096]{1,0:T(8,128)(2,1)}, u32[]{:S(2)}) copy-start(bf16[64,4096]{1,0:T(8,128)(2,1)} %param.21) | copy-start | bytes 1572868
  8.0 102.0 %all-gather.5.cloned.1.call-start = ((), (), s32[]{:S(2)}) async-start(), calls=%async_computation.4 | async-start | bytes 2359296 | tf_op jit(solution)/shard_map/all_gather | solution.py:77
  18.2 7.5 %copy-start.3 = (bf16[128,1024]{1,0:T(8,128)(2,1)S(1)}, bf16[128,1024]{1,0:T(8,128)(2,1)}, u32[]{:S(2)}) copy-start(bf16[128,1024]{1,0:T(8,128)(2,1)} %param.17) | copy-start | bytes 786436
  18.2 78.2 %all-to-all-start = ((bf16[8,32,4096]{2,1,0:T(8,128)(2,1)}), bf16[8,32,4096]{2,1,0:T(8,128)(2,1)S(1)}, u32[]{:S(2)}, u32[]{:S(2)}) async-start(bf16[8,32,4096]{2,1,0:T(8,128)(2,1)} %bitcast.20), calls=%async_computation | async-start | bytes 4194304 | tf_op jit(solution)/shard_map/all_to_all | solution.py:131
  25.6 121.7 %all-gather.3.cloned.1.call-start = ((), (), s32[]{:S(2)}) async-start(), calls=%async_computation.3 | async-start | bytes 2359296 | tf_op jit(solution)/shard_map/all_gather | solution.py:76
  26.5 138.2 %reduce-scatter.2.cloned.1.call-start = ((), (), s32[]{:S(2)}) async-start(), calls=%async_computation.5 | async-start | bytes 2621440 | tf_op jit(solution)/shard_map/reduce_scatter | solution.py:135
  107.2 2.5 %copy-start.5 = (f32[64,2]{0,1:T(2,128)S(1)}, f32[64,2]{0,1:T(2,128)}, u32[]{:S(2)}) copy-start(f32[64,2]{0,1:T(2,128)} %param.24) | copy-start | bytes 1540
  110.0 37.3 %copy-start.4 = (bf16[128,1024]{1,0:T(8,128)(2,1)S(1)}, bf16[128,1024]{1,0:T(8,128)(2,1)}, u32[]{:S(2)}) copy-start(bf16[128,1024]{1,0:T(8,128)(2,1)} %param.16) | copy-start | bytes 786436
  147.5 2.8 %copy-start = (f32[1024,4,256]{0,2,1:T(8,128)S(1)}, f32[1024,4,256]{0,2,1:T(8,128)}, u32[]{:S(2)}) copy-start(f32[1024,4,256]{0,2,1:T(8,128)} %get-tuple-element.53) | copy-start | bytes 12582916 | tf_op jit(solution)/shard_map/cond
  155.9 12.4 %copy-start.7 = (f32[4]{0:T(128)S(1)}, f32[4]{0:T(128)}, u32[]{:S(2)}) copy-start(f32[4]{0:T(128)} %param.19) | copy-start | bytes 52
  156.3 2.8 %copy-start.1 = (f32[1024,4,256]{0,2,1:T(8,128)S(1)}, f32[1024,4,256]{0,2,1:T(8,128)}, u32[]{:S(2)}) copy-start(f32[1024,4,256]{0,2,1:T(8,128)} %get-tuple-element.48) | copy-start | bytes 12582916 | tf_op jit(solution)/shard_map/cond
  164.7 4.0 %copy-start.6 = (f32[256]{0:T(256)S(1)}, f32[256]{0:T(256)}, u32[]{:S(2)}) copy-start(f32[256]{0:T(256)} %param.20) | copy-start | bytes 3076
  164.7 17.4 %all-to-all-start.1 = ((bf16[1024,8,32]{0,2,1:T(8,128)(2,1)}), bf16[1024,8,32]{0,2,1:T(8,128)(2,1)S(1)}, u32[]{:S(2)}, u32[]{:S(2)}) async-start(bf16[1024,8,32]{0,2,1:T(8,128)(2,1)} %bitcast.101), calls=%async_computation.2 | async-start | bytes 1048576 | tf_op jit(solution)/shard_map/all_to_all | solution.py:143
Sparse Core Ops, SparseCore 0:
  10.9 83.9 all-gather.4
  97.5 49.7 all-gather.2
Sparse Core Ops, SparseCore 1:
  107.3 30.1 reduce-scatter.1
where the time goes:
time: 191 us
  waiting for transfers between devices  116 us (61%)
  matrix products  26.5 us (14%)
  between operations  17.1 us (9%)
  starting transfers between devices  11 us (6%)
  local copies, waits for them, and re-layouts  10.5 us (5%)
  other arithmetic  9.63 us (5%)
    all_to_all x1, waiting for transfers between devices, local(): lax.all_to_all(outgoing, 'ep', split_axis=0, concat_axis=0, tiled=True)  69.8 us
    all_gather x1, waiting for transfers between devices, local(): key_block = lax.all_gather(key_rows, 'ep', axis=0, tiled=True)  33.2 us
    all_to_all x1, waiting for transfers between devices, local(): lax.all_to_all(summed, 'ep', split_axis=1, concat_axis=1, tiled=True)  12.6 us
    dot_general x2, matrix products, fold_block(): jnp.einsum('hmqk,khd->hmqd', weights, value_heads, precision=lax.Precisio...  9.67 us
    all_to_all x1, starting transfers between devices, local(): lax.all_to_all(outgoing, 'ep', split_axis=0, concat_axis=0, tiled=True)  7.41 us
    dot_general x1, matrix products, local(): lax.dot_general(down_local, hidden, (((0,), (1,)), ((), ())), preferred_e...  7.37 us
    dot_general x2, matrix products, fold_block(): jnp.einsum('qhmd,khmd->hmqk', query_group, key_heads, preferred_element_t...  4.85 us
    convert_element_type x1, other arithmetic, local(): value_block.reshape(key_count, head_local, VD).astype(jnp.float32)  4.08 us
  transfers between devices with their start and end apart: 5, of which 3 were waited for; matrix products, arithmetic and copies ran while one was open for 22% of the time, Pallas kernels for 0%

commit v1 on v0

--- a/solution.py
+++ b/solution.py
@@ -140,7 +140,10 @@
         scatter_dimension=0,
         tiled=True,
     )
-    returned = lax.all_to_all(summed, "ep", split_axis=1, concat_axis=1, tiled=True)
+    returned = jnp.concatenate(
+        lax.all_to_all(jnp.stack(jnp.split(summed, lax.axis_size("ep"), axis=1)), "ep", 0, 0),
+        axis=1,
+    )
     slot_ids = jnp.arange(ep_count * capacity, dtype=jnp.int32)
     combined = jnp.zeros((rows_b, returned.shape[0]), jnp.float32)
     for choice_index in range(TOP):

time: 191 us -> 203 us (1.063)
  local copies, waits for them, and re-layouts: 10.5 us -> 21.5 us
    unnamed x15 -> x22, local copies, waits for them, and re-layouts: 3.5 us -> 13.7 us
  transfers between devices with their start and end apart: 5 -> 5, of which waited for: 3 -> 3; matrix products, arithmetic and copies ran while one was open for 22% -> 21% of each run, Pallas kernels for 0% -> 0%
where the time goes in v1:
time: 203 us; the launch traced here: 202 us
  waiting for transfers between devices  116 us (57%)
  matrix products  26.3 us (13%)
  local copies, waits for them, and re-layouts  21.5 us (11%)
  between operations  17.1 us (8%)
  starting transfers between devices  11 us (5%)
  other arithmetic  9.62 us (5%)
    all_to_all x1, waiting for transfers between devices, local(): lax.all_to_all(outgoing, 'ep', split_axis=0, concat_axis=0, tiled=True)  69.8 us
    all_gather x1, waiting for transfers between devices, local(): key_block = lax.all_gather(key_rows, 'ep', axis=0, tiled=True)  33.5 us
    unnamed x22, local copies, waits for them, and re-layouts  13.7 us
    all_to_all x1, waiting for transfers between devices, local(): lax.all_to_all(jnp.stack(jnp.split(summed, lax.axis_size('ep'), axis=1)),...  12.6 us
    dot_general x2, matrix products, fold_block(): jnp.einsum('hmqk,khd->hmqd', weights, value_heads, precision=lax.Precisio...  9.67 us
    all_to_all x1, starting transfers between devices, local(): lax.all_to_all(outgoing, 'ep', split_axis=0, concat_axis=0, tiled=True)  7.41 us
    dot_general x1, matrix products, local(): lax.dot_general(down_local, hidden, (((0,), (1,)), ((), ())), preferred_e...  7.24 us
    dot_general x2, matrix products, fold_block(): jnp.einsum('qhmd,khmd->hmqk', query_group, key_heads, preferred_element_t...  4.85 us
  transfers between devices with their start and end apart: 5, of which 3 were waited for; matrix products, arithmetic and copies ran while one was open for 21% of the time, Pallas kernels for 0%

profile of v1, /device:TPU:0, one launch (start us, length us, event | category | flops | bytes accessed | tf_op | source)
XLA Modules:
  0.0 201.8 jit_solution(14192604960678532009)
XLA Ops:
  8.0 0.0 copy-start.2
  8.0 0.0 all-gather.5.cloned.1.call-start
  8.1 1.8 copy.24
  9.9 0.0 all-gather.5.cloned.1.call-update
  9.9 0.8 copy.34
  10.7 0.1 eq.45
  10.8 0.1 fusion.70
  10.9 0.2 reduce_window_sum.11
  11.1 0.2 select_reduce_fusion
  11.3 0.1 reduce_sum.71
  11.4 0.1 mul.157
  11.6 0.1 reshape.135
  11.7 1.0 scatter_custom_fusion
  12.7 1.2 fusion.42
  14.0 0.9 fusion.44
  14.9 3.2 %gather_fusion = bf16[256,4096]{1,0:T(8,128)(2,1)} fusion(bf16[64,4096]{1,0:T(8,128)(2,1)S(1)} %fusion.44, s32[1024]{0:T(1024)S(1)} %pad_clamp_fusion), kind=kCustom, calls=%fused_computation | custom fusion | bytes 4195328 | tf_op jit(solution)/shard_map/gather | solution.py:130
  18.1 7.4 %all-to-all-start = ((bf16[8,32,4096]{2,1,0:T(8,128)(2,1)}), bf16[8,32,4096]{2,1,0:T(8,128)(2,1)S(1)}, u32[]{:S(2)}, u32[]{:S(2)}) async-start(bf16[8,32,4096]{2,1,0:T(8,128)(2,1)} %bitcast.20), calls=%async_computation | async-start | bytes 4194304 | tf_op jit(solution)/shard_map/all_to_all | solution.py:131
  25.5 0.0 all-gather.3.cloned.1.call-start
  25.6 0.8 copy.23
  26.4 0.0 all-gather.3.cloned.1.call-update
  26.5 0.0 reduce-scatter.2.cloned.1.call-start
  26.5 69.8 %all-to-all-done = bf16[8,32,4096]{2,1,0:T(8,128)(2,1)S(1)} async-done(((bf16[8,32,4096]{2,1,0:T(8,128)(2,1)}), bf16[8,32,4096]{2,1,0:T(8,128)(2,1)S(1)}, u32[]{:S(2)}, u32[]{:S(2)}) %all-to-all-start) | async-done | bytes 2097184 | tf_op jit(solution)/shard_map/all_to_all | solution.py:131
  96.3 3.4 %fusion.32 = f32[256,512]{1,0:T(8,128)S(1)} fusion(bf16[256,4096]{1,0:T(8,128)(2,1)S(1)} %bitcast.132, bf16[1,4096,512]{2,1,0:T(8,128)(2,1)} %param.25), kind=kOutput, calls=%fused_computation.43 | convolution fusion | flops 1073741824 | bytes 6815744 | tf_op jit(solution)/shard_map/dot_general | solution.py:132
  99.7 7.2 %fusion.28 = bf16[4096,256]{0,1:T(8,128)(2,1)} fusion(bf16[1,512,4096]{2,1,0:T(8,128)(2,1)} %param.27, bf16[256,4096]{1,0:T(8,128)(2,1)S(1)} %bitcast.133, bf16[1,4096,512]{2,1,0:T(8,128)(2,1)} %param.26, f32[256,512]{1,0:T(8,128)S(1)} %fusion.32), kind=kOutput, calls=%fused_computation.39 | convolution fusion | flops 2149318656 | bytes 13107200 | tf_op jit(solution)/shard_map/dot_general | solution.py:136
  107.0 0.0 reduce-scatter.2.cloned.1.call-update
  107.0 0.6 slice.50
  108.2 0.6 slice.55
  109.6 0.2 slice_reduce_fusion
  109.8 0.0 all-gather.5.cloned.1.call-done
  109.8 0.0 copy-start.4
  109.8 4.1 %convert.3 = f32[1024,4,256]{0,2,1:T(8,128)} convert(bf16[1024,4,256]{0,2,1:T(8,128)(2,1)} %bitcast.131) | non-fusion elementwise | flops 1048576 | bytes 6291456 | tf_op jit(solution)/shard_map/convert_element_type | solution.py:80
  113.9 33.5 %all-gather.3.cloned.1.call-done = bf16[1024,1024]{0,1:T(8,128)(2,1)} async-done(((bf16[128,1024]{0,1:T(8,128)(2,1)}), bf16[1024,1024]{0,1:T(8,128)(2,1)}) %all-gather.3.cloned.1.call-update) | async-done | bytes 2097168 | tf_op jit(solution)/shard_map/all_gather | solution.py:76
  147.5 0.0 copy-done.4
  147.5 8.2 %conditional.2 = (f32[4,2,64]{2,1,0:T(2,128)S(1)}, f32[4,2,64,256]{3,2,1,0:T(8,128)S(1)}) conditional(s32[]{:T(128)} %bitcast.2, () %tuple.24, (s32[1024]{0:T(1024)S(1)}, s32[64]{0:T(128)S(1)}, bf16[128,1024]{1,0:T(8,128)(2,1)S(1)}, bf16[1024,4,2,128]{0,3,2,1:T(8,128)(2,1)}, f32[1024,4,256]{0,2,1:T(8,128)}) %tuple.56), branch_computations={%region_0.0_spmd, %region_1.4_spmd} | conditional | flops 1751186944 | bytes 30818604 | solution.py:87
  147.5 0.1 broadcast_compare_fusion
  147.6 0.1 reshape.110
  147.7 0.0 copy-start
  147.7 2.4 %fusion.2 = (f32[4,2,64]{2,1,0:T(2,128)S(1)}, f32[4,2,64,1024]{3,2,1,0:T(8,128)S(1)}) fusion(pred[64,1024]{1,0:T(8,128)(4,1)S(1)} %broadcast_compare_fusion, bf16[1024,4,2,128]{0,3,2,1:T(8,128)(2,1)} %get-tuple-element.47, bf16[64,4,2,128]{3,2,1,0:T(2,128)(2,1)S(1)} %reshape.110), kind=kOutput, calls=%fused_computation.6 | convolution fusion | flops 135790080 | bytes 4392960 | tf_op jit(solution)/shard_map/cond/branch_1_fun/qhmd,khmd->hmqk/dot_general | solution.py:27
  150.1 0.7 fusion.3
  150.8 4.8 %fusion = f32[4,2,64,256]{3,2,1,0:T(8,128)S(1)} fusion(f32[1024,4,256]{0,2,1:T(8,128)S(1)} %copy-done, f32[4,2,64,1024]{3,2,1,0:T(8,128)S(1)} %get-tuple-element.61, f32[4,2,64]{2,1,0:T(2,128)S(1)} %broadcast_maximum_fusion, pred[64,1024]{1,0:T(8,128)(4,1)S(1)} %broadcast_compare_fusion), kind=kOutput, calls=%fused_computation.2 | convolution fusion | flops 1612709888 | bytes 6883328 | tf_op jit(solution)/shard_map/cond/branch_1_fun/hmqk,khd->hmqd/dot_general | solution.py:34
  155.7 8.4 %conditional.3 = (f32[4,2,64]{2,1,0:T(2,128)S(1)}, f32[4,2,64,256]{3,2,1,0:T(8,128)S(1)}) conditional(s32[]{:T(128)} %bitcast.10, () %tuple.26, (s32[1024]{0:T(1024)S(1)}, s32[64]{0:T(128)S(1)}, bf16[128,1024]{1,0:T(8,128)(2,1)S(1)}, bf16[1024,4,2,128]{0,3,2,1:T(8,128)(2,1)}, f32[1024,4,256]{0,2,1:T(8,128)}) %tuple.57), branch_computations={%region_5.6_spmd, %region_6.9_spmd} | conditional | flops 1751186944 | bytes 30818604 | solution.py:87
  155.9 0.1 broadcast_compare_fusion.1
  156.0 0.1 reshape.111
  156.1 2.4 %fusion.16 = (f32[4,2,64]{2,1,0:T(2,128)S(1)}, f32[4,2,64,1024]{3,2,1,0:T(8,128)S(1)}) fusion(pred[64,1024]{1,0:T(8,128)(4,1)S(1)} %broadcast_compare_fusion.1, bf16[1024,4,2,128]{0,3,2,1:T(8,128)(2,1)} %get-tuple-element.52, bf16[64,4,2,128]{3,2,1,0:T(2,128)(2,1)S(1)} %reshape.111), kind=kOutput, calls=%fused_computation.24 | convolution fusion | flops 135790080 | bytes 4392960 | tf_op jit(solution)/shard_map/cond/branch_1_fun/qhmd,khmd->hmqk/dot_general | solution.py:27
  158.5 0.7 fusion.17
  159.3 4.8 %fusion.14 = f32[4,2,64,256]{3,2,1,0:T(8,128)S(1)} fusion(f32[1024,4,256]{0,2,1:T(8,128)S(1)} %copy-done.1, f32[4,2,64,1024]{3,2,1,0:T(8,128)S(1)} %get-tuple-element.63, f32[4,2,64]{2,1,0:T(2,128)S(1)} %broadcast_maximum_fusion.1, pred[64,1024]{1,0:T(8,128)(4,1)S(1)} %broadcast_compare_fusion.1), kind=kOutput, calls=%fused_computation.20 | convolution fusion | flops 1612709888 | bytes 6883328 | tf_op jit(solution)/shard_map/cond/branch_1_fun/hmqk,khd->hmqd/dot_general | solution.py:34
  164.1 0.0 copy-start.7
  164.1 0.0 copy-start.6
  164.1 0.0 reduce-scatter.2.cloned.1.call-done
  164.2 1.5 fusion.69
  165.6 1.5 fusion.68
  167.1 1.5 fusion.67
  168.6 1.5 fusion.66
  170.0 1.5 fusion.65
  171.5 1.5 fusion.64
  172.9 1.5 fusion.63
  174.4 1.5 fusion.62
  175.9 3.5 %all-to-all-start.1 = ((bf16[8,1024,32]{1,2,0:T(8,128)(2,1)}), bf16[8,1024,32]{1,2,0:T(8,128)(2,1)S(1)}, u32[]{:S(2)}, u32[]{:S(2)}) async-start(bf16[8,1024,32]{1,2,0:T(8,128)(2,1)} %fusion.62), calls=%async_computation.2 | async-start | bytes 1048576 | tf_op jit(solution)/shard_map/all_to_all | solution.py:144
  179.4 0.3 multiply_reduce_fusion.1
  179.8 0.1 fusion.60
  179.9 0.7 pad_maximum_fusion
  180.7 12.6 %all-to-all-done.1 = bf16[8,1024,32]{1,2,0:T(8,128)(2,1)S(1)} async-done(((bf16[8,1024,32]{1,2,0:T(8,128)(2,1)}), bf16[8,1024,32]{1,2,0:T(8,128)(2,1)S(1)}, u32[]{:S(2)}, u32[]{:S(2)}) %all-to-all-start.1) | async-done | bytes 524320 | tf_op jit(solution)/shard_map/all_to_all | solution.py:144
  193.2 0.2 convolution_multiply_fusion.1
  193.5 0.9 fusion.41
  (33 shorter events, 0.2 us)
Async XLA Ops:
  8.0 6.0 %copy-start.2 = (bf16[64,4096]{1,0:T(8,128)(2,1)S(1)}, bf16[64,4096]{1,0:T(8,128)(2,1)}, u32[]{:S(2)}) copy-start(bf16[64,4096]{1,0:T(8,128)(2,1)} %param.21) | copy-start | bytes 1572868
  8.0 101.8 %all-gather.5.cloned.1.call-start = ((), (), s32[]{:S(2)}) async-start(), calls=%async_computation.4 | async-start | bytes 2359296 | tf_op jit(solution)/shard_map/all_gather | solution.py:77
  18.1 7.5 %copy-start.3 = (bf16[128,1024]{1,0:T(8,128)(2,1)S(1)}, bf16[128,1024]{1,0:T(8,128)(2,1)}, u32[]{:S(2)}) copy-start(bf16[128,1024]{1,0:T(8,128)(2,1)} %param.17) | copy-start | bytes 786436
  18.1 78.2 %all-to-all-start = ((bf16[8,32,4096]{2,1,0:T(8,128)(2,1)}), bf16[8,32,4096]{2,1,0:T(8,128)(2,1)S(1)}, u32[]{:S(2)}, u32[]{:S(2)}) async-start(bf16[8,32,4096]{2,1,0:T(8,128)(2,1)} %bitcast.20), calls=%async_computation | async-start | bytes 4194304 | tf_op jit(solution)/shard_map/all_to_all | solution.py:131
  25.5 121.9 %all-gather.3.cloned.1.call-start = ((), (), s32[]{:S(2)}) async-start(), calls=%async_computation.3 | async-start | bytes 2359296 | tf_op jit(solution)/shard_map/all_gather | solution.py:76
  26.5 137.7 %reduce-scatter.2.cloned.1.call-start = ((), (), s32[]{:S(2)}) async-start(), calls=%async_computation.5 | async-start | bytes 2621440 | tf_op jit(solution)/shard_map/reduce_scatter | solution.py:135
  107.0 2.6 %copy-start.5 = (f32[64,2]{0,1:T(2,128)S(1)}, f32[64,2]{0,1:T(2,128)}, u32[]{:S(2)}) copy-start(f32[64,2]{0,1:T(2,128)} %param.24) | copy-start | bytes 1540
  109.8 37.7 %copy-start.4 = (bf16[128,1024]{1,0:T(8,128)(2,1)S(1)}, bf16[128,1024]{1,0:T(8,128)(2,1)}, u32[]{:S(2)}) copy-start(bf16[128,1024]{1,0:T(8,128)(2,1)} %param.16) | copy-start | bytes 786436
  147.7 3.2 %copy-start = (f32[1024,4,256]{0,2,1:T(8,128)S(1)}, f32[1024,4,256]{0,2,1:T(8,128)}, u32[]{:S(2)}) copy-start(f32[1024,4,256]{0,2,1:T(8,128)} %get-tuple-element.48) | copy-start | bytes 12582916 | tf_op jit(solution)/shard_map/cond
  156.1 3.2 %copy-start.1 = (f32[1024,4,256]{0,2,1:T(8,128)S(1)}, f32[1024,4,256]{0,2,1:T(8,128)}, u32[]{:S(2)}) copy-start(f32[1024,4,256]{0,2,1:T(8,128)} %get-tuple-element.53) | copy-start | bytes 12582916 | tf_op jit(solution)/shard_map/cond
  164.1 15.3 %copy-start.7 = (f32[4]{0:T(128)S(1)}, f32[4]{0:T(128)}, u32[]{:S(2)}) copy-start(f32[4]{0:T(128)} %param.19) | copy-start | bytes 52
  164.1 15.6 %copy-start.6 = (f32[256]{0:T(256)S(1)}, f32[256]{0:T(256)}, u32[]{:S(2)}) copy-start(f32[256]{0:T(256)} %param.20) | copy-start | bytes 3076
  175.9 17.4 %all-to-all-start.1 = ((bf16[8,1024,32]{1,2,0:T(8,128)(2,1)}), bf16[8,1024,32]{1,2,0:T(8,128)(2,1)S(1)}, u32[]{:S(2)}, u32[]{:S(2)}) async-start(bf16[8,1024,32]{1,2,0:T(8,128)(2,1)} %fusion.62), calls=%async_computation.2 | async-start | bytes 1048576 | tf_op jit(solution)/shard_map/all_to_all | solution.py:144
Sparse Core Ops, SparseCore 0:
  10.9 83.9 all-gather.4
  97.4 49.9 all-gather.2
Sparse Core Ops, SparseCore 1:
  107.1 30.1 reduce-scatter.1
